TPU v7x, 32 devices: a whole 2x2x4 slice. The times are simulated.
32 devices in a mesh: ep: 8 (over z, core), tp: 4 (over y, x).
Axes of the slice: x: 2, y: 2, z: 4, core: 2. Of those that a mesh axis runs over, the one named last changes fastest.
Arguments:
- compressed_query: bfloat16 [1024, 1536], P('ep'), may hold values from -6 to 6
- compressed_key_value: bfloat16 [1024, 512], P('ep'), may hold values from -6 to 6
- rotary_key: bfloat16 [1024, 32], P('ep'), may hold values from -600 to 600
- query_norm_scale: float32 [1536], replicated, may hold values from 0.1 to 1.9
- context_norm_scale: float32 [512], replicated, may hold values from 0.1 to 1.9
- query_plain_weight: bfloat16 [1536, 1024], P(None, 'tp'), may hold values from -0.375 to 0.375
- query_rotary_weight: bfloat16 [1536, 512], P(None, 'tp'), may hold values from -0.375 to 0.375
- key_up_weight: bfloat16 [512, 1024], P(None, 'tp'), may hold values from -0.25 to 0.25
- value_up_weight: bfloat16 [512, 1024], P(None, 'tp'), may hold values from -0.25 to 0.25
- output_weight: bfloat16 [1024, 2048], P(None, 'tp'), may hold values from -0.75 to 0.75
- mixture_input: bfloat16 [1024, 2048], P('ep'), may hold values from -6 to 6
- mixture_gain: float32 [2048], replicated, may hold values from 0.1 to 1.9
- routes: int32 [1024, 2], P('ep'), may hold values from 0 to 7, all different within a row; in each aligned block of 128 rows (0 to 127, 128 to 255, ...) at most 48 rows name the same one
- route_weight: float32 [1024, 2], P('ep'), may hold values from 0.2 to 2
- expert_gate: bfloat16 [8, 2048, 4096], P('ep', None, 'tp'), may hold values from -0.125 to 0.125
- expert_up: bfloat16 [8, 2048, 4096], P('ep', None, 'tp'), may hold values from -0.125 to 0.125
- expert_down: bfloat16 [8, 4096, 2048], P('ep', None, 'tp'), may hold values from -0.09375 to 0.09375
- shared_gate: bfloat16 [2048, 512], P(None, 'tp'), may hold values from -0.125 to 0.125
- shared_up: bfloat16 [2048, 512], P(None, 'tp'), may hold values from -0.125 to 0.125
- shared_down: bfloat16 [512, 2048], P(None, 'tp'), may hold values from -0.25 to 0.25
Outputs:
- attended: bfloat16 [1024, 2048], P('ep', 'tp')
- combined: bfloat16 [1024, 2048], P('ep', 'tp')
Inputs may be any that keep to these rules, and one draw needn't show every extreme that they name: `routes`: in the rows of each index of ep, no expert is named more than 48 times, a bound that some block reaches there.
All inputs are finite; a program needn't handle non-finite values.
Results may differ from a plain program's by a relative error of at most 0.012.
The roundings to bfloat16 on the way count: a program that leaves them out, or rounds other values in their place, can miss the bound.
Values may be sent and summed in bfloat16 or wider, within the bound.
No kernel may reach another device: no remote copies, remote signals or barrier semaphores. Data moves between devices by JAX's collectives and lax.ppermute only.
A program may use at most 64 MiB of HBM per device.

v0:
```python
import math
import jax
import jax.numpy as jnp
from jax import lax
from jax.sharding import PartitionSpec as P

PLAIN_HEAD_SIZE = 64
ROTARY_SIZE = 32
VALUE_HEAD_SIZE = 64
TOPK = 2


def normed_rows(values, scaling):
    floats = values.astype(jnp.float32)
    return floats * lax.rsqrt(jnp.mean(floats * floats, axis=-1, keepdims=True) + 1e-06) * scaling


def rotary_tables(positions):
    inverse = 1.0 / 10000.0 ** (jnp.arange(0, ROTARY_SIZE, 2, dtype=jnp.float32) / ROTARY_SIZE)
    angles = positions.astype(jnp.float32)[:, None] * inverse[None, :]
    return (jnp.cos(angles), jnp.sin(angles))


def rotate(vectors, cosine, sine_part):
    half_width = vectors.shape[-1] // 2
    front_half = vectors[..., :half_width]
    back_half = vectors[..., half_width:]
    return jnp.concatenate(
        [front_half * cosine - back_half * sine_part, front_half * sine_part + back_half * cosine],
        axis=-1,
    )


def fold_blocks(carry_state, members, handle):
    length = members[0].shape[0]
    block_rows = math.gcd(length, 2048)

    def advance(block_index, carried):
        sliced = tuple(
            (
                lax.dynamic_slice_in_dim(member, block_index * block_rows, block_rows, 0)
                for member in members
            )
        )
        return handle(carried, sliced, block_index * block_rows)

    return lax.fori_loop(0, length // block_rows, advance, carry_state)


def per_device(
    compressed_query,
    compressed_key_value,
    rotary_key,
    query_norm_scale,
    context_norm_scale,
    query_plain_weight,
    query_rotary_weight,
    key_up_weight,
    value_up_weight,
    output_weight,
    mixture_input,
    mixture_gain,
    routes,
    route_weight,
    expert_gate,
    expert_up,
    expert_down,
    shared_gate,
    shared_up,
    shared_down,
):
    tokens = compressed_query.shape[0]
    heads_here = query_plain_weight.shape[1] // PLAIN_HEAD_SIZE
    offset = lax.axis_index("ep") * tokens
    cosine, sine_part = rotary_tables(offset + jnp.arange(tokens, dtype=jnp.int32))
    compressed = normed_rows(compressed_query, query_norm_scale).astype(jnp.bfloat16)
    query_nope = jnp.dot(compressed, query_plain_weight, preferred_element_type=jnp.float32)
    query_nope = query_nope.astype(jnp.bfloat16).reshape(tokens, heads_here, PLAIN_HEAD_SIZE)
    query_turn = jnp.dot(compressed, query_rotary_weight, preferred_element_type=jnp.float32)
    query_turn = query_turn.reshape(tokens, heads_here, ROTARY_SIZE)
    query_rot = rotate(query_turn, cosine[:, None, :], sine_part[:, None, :])
    context = normed_rows(compressed_key_value, context_norm_scale).astype(jnp.bfloat16)
    scale = (PLAIN_HEAD_SIZE + ROTARY_SIZE) ** (-0.5)
    start_state = (
        jnp.full((heads_here, tokens), -1e30, jnp.float32),
        jnp.zeros((heads_here, tokens), jnp.float32),
        jnp.zeros((heads_here, tokens, VALUE_HEAD_SIZE), jnp.float32),
    )

    def attend(carry_state, sliced, first_row):
        key_rows, value_rows, raw_turn = sliced
        count = raw_turn.shape[0]
        key_cos, key_sin = rotary_tables(first_row + jnp.arange(count, dtype=jnp.int32))
        turned = rotate(raw_turn.astype(jnp.float32), key_cos, key_sin)
        running_max, running_total, running_sum = carry_state
        key_heads = key_rows.reshape(count, heads_here, PLAIN_HEAD_SIZE)
        value_heads = value_rows.reshape(count, heads_here, VALUE_HEAD_SIZE)
        scores = (
            jnp.einsum("qhe,khe->hqk", query_nope, key_heads, preferred_element_type=jnp.float32)
            + jnp.einsum("qhr,kr->hqk", query_rot, turned, precision=lax.Precision.HIGHEST)
        ) * scale
        new_max = jnp.maximum(running_max, jnp.max(scores, axis=-1))
        factor = jnp.exp(running_max - new_max)
        weights = jnp.exp(scores - new_max[..., None])
        running_total = running_total * factor + jnp.sum(weights, axis=-1)
        running_sum = running_sum * factor[..., None] + jnp.einsum(
            "hqk,khe->hqe",
            weights.astype(jnp.bfloat16),
            value_heads,
            preferred_element_type=jnp.float32,
        )
        return (new_max, running_total, running_sum)

    def expand(carry_state, sliced, first_row):
        latent_rows, raw_turn = sliced
        key_rows = jnp.dot(latent_rows, key_up_weight, preferred_element_type=jnp.float32).astype(
            jnp.bfloat16
        )
        value_rows = jnp.dot(
            latent_rows, value_up_weight, preferred_element_type=jnp.float32
        ).astype(jnp.bfloat16)
        return attend(carry_state, (key_rows, value_rows, raw_turn), first_row)

    final_state = fold_blocks(
        start_state,
        (
            lax.all_gather(context, "ep", axis=0, tiled=True),
            lax.all_gather(rotary_key, "ep", axis=0, tiled=True),
        ),
        expand,
    )
    heads_out = final_state[2] / final_state[1][..., None]
    heads_out = (
        heads_out.transpose(1, 0, 2)
        .reshape(tokens, heads_here * VALUE_HEAD_SIZE)
        .astype(jnp.bfloat16)
    )
    all_heads = lax.all_gather(heads_out, "tp", axis=1, tiled=True)
    attended = jnp.dot(all_heads, output_weight, preferred_element_type=jnp.float32).astype(
        jnp.bfloat16
    )
    floats = mixture_input.astype(jnp.float32)
    centred = floats - jnp.mean(floats, axis=-1, keepdims=True)
    normed = (
        centred
        * lax.rsqrt(jnp.mean(centred * centred, axis=-1, keepdims=True) + 1e-05)
        * mixture_gain
    ).astype(jnp.bfloat16)
    experts = lax.axis_size("ep")
    rows_here = mixture_input.shape[0]
    model_width = normed.shape[1]
    capacity = rows_here * TOPK * 3 // (2 * experts)
    flat_routes = routes.reshape(-1)
    one_hot = (flat_routes[:, None] == jnp.arange(experts, dtype=jnp.int32)[None, :]).astype(
        jnp.int32
    )
    ranks = jnp.sum(one_hot * (jnp.cumsum(one_hot, axis=0) - 1), axis=1)
    slots = flat_routes * capacity + ranks
    owners = jnp.full((experts * capacity,), rows_here, jnp.int32)
    owners = owners.at[slots].set(jnp.arange(rows_here * TOPK, dtype=jnp.int32) // TOPK)
    padded = jnp.concatenate([normed, jnp.zeros((1, model_width), jnp.bfloat16)], axis=0)
    outgoing = padded[owners].reshape(experts, capacity, model_width)
    arrived = lax.all_to_all(outgoing, "ep", split_axis=0, concat_axis=0, tiled=True).reshape(
        experts * capacity, model_width
    )
    hidden = (
        jax.nn.silu(jnp.dot(arrived, expert_gate[0], preferred_element_type=jnp.float32))
        * jnp.dot(arrived, expert_up[0], preferred_element_type=jnp.float32)
    ).astype(jnp.bfloat16)
    shared_hidden = (
        jax.nn.silu(jnp.dot(normed, shared_gate, preferred_element_type=jnp.float32))
        * jnp.dot(normed, shared_up, preferred_element_type=jnp.float32)
    ).astype(jnp.bfloat16)
    all_hidden, all_shared = (
        lax.all_gather(hidden, "tp", axis=1, tiled=True),
        lax.all_gather(shared_hidden, "tp", axis=1, tiled=True),
    )
    expert_rows = jnp.dot(all_hidden, expert_down[0], preferred_element_type=jnp.float32).astype(
        jnp.bfloat16
    )
    features = expert_rows.shape[1]
    returned = lax.all_to_all(
        expert_rows.reshape(experts, capacity, features),
        "ep",
        split_axis=0,
        concat_axis=0,
        tiled=True,
    )
    picked = returned.reshape(experts * capacity, features)[slots]
    picked = picked.astype(jnp.float32).reshape(rows_here, TOPK, features)
    routed = jnp.sum(picked * route_weight[:, :, None], axis=1)
    combined = (
        jnp.dot(all_shared, shared_down, preferred_element_type=jnp.float32) + routed
    ).astype(jnp.bfloat16)
    return (attended, combined)


def solution(mesh):
    in_specs = (
        P("ep", None),
        P("ep", None),
        P("ep", None),
        P(),
        P(),
        P(None, "tp"),
        P(None, "tp"),
        P(None, "tp"),
        P(None, "tp"),
        P(None, "tp"),
        P("ep", None),
        P(),
        P("ep", None),
        P("ep", None),
        P("ep", None, "tp"),
        P("ep", None, "tp"),
        P("ep", None, "tp"),
        P(None, "tp"),
        P(None, "tp"),
        P(None, "tp"),
    )
    out_specs = (P("ep", "tp"), P("ep", "tp"))
    return jax.shard_map(
        per_device, mesh=mesh, in_specs=in_specs, out_specs=out_specs, check_vma=False
    )
```

profile of v0, /device:TPU:0, one launch (start us, length us, event | category | flops | bytes accessed | tf_op | source)
XLA Modules:
  0.0 154.8 jit_solution(1504360362727506415)
XLA Ops:
  10.2 1.4 scatter_custom_fusion
  11.7 1.2 convert_reduce_fusion
  12.9 1.3 fusion.21
  14.2 1.4 fusion.23
  15.7 3.1 %gather_fusion = bf16[384,2048]{1,0:T(8,128)(2,1)} fusion(bf16[129,2048]{1,0:T(8,128)(2,1)S(1)} %concatenate.12, s32[1024]{0:T(1024)S(1)} %pad_clamp_fusion.1), kind=kCustom, calls=%fused_computation | custom fusion | bytes 3147264 | tf_op jit(solution)/shard_map/gather | solution.py:162
  18.8 6.5 %all-to-all-start = ((bf16[8,48,2048]{2,1,0:T(8,128)(2,1)}), bf16[8,48,2048]{2,1,0:T(8,128)(2,1)S(1)}, u32[]{:S(2)}, u32[]{:S(2)}) async-start(bf16[8,48,2048]{2,1,0:T(8,128)(2,1)} %bitcast.14), calls=%async_computation | async-start | bytes 3145728 | tf_op jit(solution)/shard_map/all_to_all | solution.py:163
  26.3 45.2 %all-to-all-done = bf16[8,48,2048]{2,1,0:T(8,128)(2,1)S(1)} async-done(((bf16[8,48,2048]{2,1,0:T(8,128)(2,1)}), bf16[8,48,2048]{2,1,0:T(8,128)(2,1)S(1)}, u32[]{:S(2)}, u32[]{:S(2)}) %all-to-all-start) | async-done | bytes 1572896 | tf_op jit(solution)/shard_map/all_to_all | solution.py:163
  71.5 4.1 %fusion.4 = f32[384,1024]{1,0:T(8,128)S(1)} fusion(bf16[384,2048]{1,0:T(8,128)(2,1)S(1)} %bitcast.76, bf16[1,2048,1024]{2,1,0:T(8,128)(2,1)} %param.34), kind=kOutput, calls=%fused_computation.7 | convolution fusion | flops 1610612736 | bytes 7340032 | tf_op jit(solution)/shard_map/dot_general | solution.py:167
  75.7 2.9 %multiply_convert_fusion = bf16[384,1024]{1,0:T(8,128)(2,1)} fusion(f32[384,1024]{1,0:T(8,128)S(1)} %fusion.4, bf16[384,2048]{1,0:T(8,128)(2,1)S(1)} %bitcast.77, bf16[1,2048,1024]{2,1,0:T(8,128)(2,1)S(1)} %copy-done.13), kind=kOutput, calls=%fused_computation.14 | convolution fusion | flops 1612972032 | bytes 8126464 | tf_op jit(solution)/shard_map/dot_general | solution.py:168
  78.8 1.6 %convolution_convert_fusion.3 = bf16[128,256]{1,0:T(8,128)(2,1)S(1)} fusion(bf16[1536,256]{1,0:T(8,128)(2,1)} %param.25, bf16[128,1536]{1,0:T(8,128)(2,1)S(1)} %copy-done.6, f32[1536]{0:T(1024)S(1)} %copy-done.16, f32[128]{0:T(128)S(1)} %add_rsqrt_fusion.2), kind=kOutput, calls=%fused_computation.28 | convolution fusion | flops 101482496 | bytes 1251840 | tf_op jit(solution)/shard_map/dot_general | solution.py:77
  80.5 12.8 %all_gather.16 = bf16[1024,32]{0,1:T(8,128)(2,1)S(1)} all-gather(bf16[128,32]{0,1:T(8,128)(2,1)S(1)} %copy-done.10), channel_id=1, replica_groups=mesh['ep'=8,'tp'=4] {'ep'}, dimensions={0}, use_global_device_ids=true | all-gather | bytes 73728 | tf_op jit(solution)/shard_map/all_gather | solution.py:128
  94.7 9.3 %all_gather.18 = bf16[128,512]{1,0:T(8,128)(2,1)} all-gather(bf16[128,128]{1,0:T(8,128)(2,1)S(1)} %fusion.20), channel_id=1, replica_groups=mesh['ep'=8,'tp'=4] {'tp'}, dimensions={1}, use_global_device_ids=true | all-gather | bytes 163840 | tf_op jit(solution)/shard_map/all_gather | solution.py:176
  105.6 1.7 %convolution_convert_fusion.1 = bf16[1024,256]{0,1:T(8,128)(2,1)S(1)} fusion(bf16[1024,512]{1,0:T(8,128)(2,1)} %all-gather.3.cloned.1.call-done, bf16[512,256]{1,0:T(8,128)(2,1)S(1)} %copy-done.7), kind=kOutput, calls=%fused_computation.18 | convolution fusion | flops 268697600 | bytes 1835008 | tf_op jit(solution)/shard_map/while/body/eval_jaxpr/dot_general | solution.py:116
  107.8 2.0 %fusion.51 = (f32[4,128]{1,0:T(4,128)S(1)}, f32[4,128,1024]{2,1,0:T(8,128)S(1)}) fusion(f32[4,128,1024]{2,1,0:T(8,128)S(1)} %fusion.52, f32[128,4,16]{0,2,1:T(8,128)S(1)} %get-tuple-element.27, f32[128,4,16]{0,2,1:T(8,128)S(1)} %get-tuple-element.26, f32[1024,16]{0,1:T(8,128)S(1)} %get-tuple-element.25, f32[1024,16]{0,1:T(8,128)S(1)} %get-tuple-element.24), kind=kOutput, calls=%fused_computation.94 | convolution fusion | flops 202948096 | bytes 4392960 | tf_op jit(solution)/shard_map/while/body/eval_jaxpr/qhr,kr->hqk/dot_general | solution.py:100
  111.1 1.3 convolution_convert_fusion
  112.3 9.5 %all-gather.5.cloned.1.call-done = bf16[384,4096]{1,0:T(8,128)(2,1)} async-done(((bf16[384,1024]{1,0:T(8,128)(2,1)}), bf16[384,4096]{1,0:T(8,128)(2,1)}) %all-gather.5.cloned.1.call-update) | async-done | bytes 3145744 | tf_op jit(solution)/shard_map/all_gather | solution.py:175
  121.8 5.7 %fusion.11 = bf16[384,512]{1,0:T(8,128)(2,1)} fusion(bf16[384,4096]{1,0:T(8,128)(2,1)} %all-gather.5.cloned.1.call-done, bf16[1,4096,512]{2,1,0:T(8,128)(2,1)} %param.36), kind=kOutput, calls=%fused_computation.19 | convolution fusion | flops 1610809344 | bytes 7733248 | tf_op jit(solution)/shard_map/dot_general | solution.py:178
  127.5 4.6 %all-to-all-start.1 = ((bf16[8,48,512]{2,1,0:T(8,128)(2,1)}), bf16[8,48,512]{2,1,0:T(8,128)(2,1)S(1)}, u32[]{:S(2)}, u32[]{:S(2)}) async-start(bf16[8,48,512]{2,1,0:T(8,128)(2,1)} %bitcast.78), calls=%async_computation.1 | async-start | bytes 786432 | tf_op jit(solution)/shard_map/all_to_all | solution.py:182
  132.1 1.6 %fusion.19 = bf16[128,4,64]{0,2,1:T(8,128)(2,1)S(1)} fusion(bf16[1024,4,64]{0,2,1:T(8,128)(2,1)} %bitcast.74, f32[4,128,1024]{2,1,0:T(8,128)S(1)} %get-tuple-element.44, f32[4,128]{1,0:T(4,128)S(1)} %get-tuple-element.29, f32[128,4]{0,1:T(4,128)S(1)} %bitcast_add_fusion.1, f32[128,4]{0,1:T(4,128)S(1)} %get-tuple-element.28), kind=kOutput, calls=%fused_computation.29 | convolution fusion | flops 68255744 | bytes 2693120 | tf_op jit(solution)/shard_map/while/body/eval_jaxpr/hqk,khe->hqe/dot_general | solution.py:106
  133.8 8.9 %all_gather.17 = bf16[128,1024]{0,1:T(8,128)(2,1)S(1)} all-gather(bf16[128,256]{0,1:T(8,128)(2,1)S(1)} %bitcast.79), channel_id=1, replica_groups=mesh['ep'=8,'tp'=4] {'tp'}, dimensions={1}, use_global_device_ids=true | all-gather | bytes 327680 | tf_op jit(solution)/shard_map/all_gather | solution.py:138
  142.7 1.0 convolution_convert_fusion.2
  143.7 1.0 all-to-all-done.1
  144.6 1.3 gather_fusion.1
  147.0 0.9 fusion.16
  (82 shorter events, 10.0 us)
Async XLA Ops:
  7.2 135.5 %copy-start = (bf16[1024,512]{1,0:T(8,128)(2,1)S(1)}, bf16[1024,512]{1,0:T(8,128)(2,1)}, u32[]{:S(2)}) copy-start(bf16[1024,512]{1,0:T(8,128)(2,1)} %param.29) | copy-start | bytes 3145732
  18.8 6.5 %copy-start.4 = (bf16[128,512]{1,0:T(8,128)(2,1)S(1)}, bf16[128,512]{1,0:T(8,128)(2,1)}, u32[]{:S(2)}) copy-start(bf16[128,512]{1,0:T(8,128)(2,1)} %param.21) | copy-start | bytes 393220
  18.8 6.7 %copy-start.11 = (f32[512]{0:T(512)S(1)}, f32[512]{0:T(512)}, u32[]{:S(2)}) copy-start(f32[512]{0:T(512)} %param.24) | copy-start | bytes 6148
  18.8 52.7 %all-to-all-start = ((bf16[8,48,2048]{2,1,0:T(8,128)(2,1)}), bf16[8,48,2048]{2,1,0:T(8,128)(2,1)S(1)}, u32[]{:S(2)}, u32[]{:S(2)}) async-start(bf16[8,48,2048]{2,1,0:T(8,128)(2,1)} %bitcast.14), calls=%async_computation | async-start | bytes 3145728 | tf_op jit(solution)/shard_map/all_to_all | solution.py:163
  25.3 80.2 %all-gather.3.cloned.1.call-start = ((), (), s32[]{:S(2)}) async-start(), calls=%async_computation.2 | async-start | bytes 1179648 | tf_op jit(solution)/shard_map/all_gather | solution.py:127
  26.3 95.6 %all-gather.5.cloned.1.call-start = ((), (), s32[]{:S(2)}) async-start(), calls=%async_computation.3 | async-start | bytes 3932160 | tf_op jit(solution)/shard_map/all_gather | solution.py:175
  71.5 4.2 %copy-start.13 = (bf16[1,2048,1024]{2,1,0:T(8,128)(2,1)S(1)}, bf16[1,2048,1024]{2,1,0:T(8,128)(2,1)}, u32[]{:S(2)}) copy-start(bf16[1,2048,1024]{2,1,0:T(8,128)(2,1)} %param.35) | copy-start | bytes 12582916
  75.7 2.9 %copy-start.6 = (bf16[128,1536]{1,0:T(8,128)(2,1)S(1)}, bf16[128,1536]{1,0:T(8,128)(2,1)}, u32[]{:S(2)}) copy-start(bf16[128,1536]{1,0:T(8,128)(2,1)} %param.20) | copy-start | bytes 1179652
  75.7 3.1 %copy-start.16 = (f32[1536]{0:T(1024)S(1)}, f32[1536]{0:T(1024)}, u32[]{:S(2)}) copy-start(f32[1536]{0:T(1024)} %param.23) | copy-start | bytes 18436
  78.6 1.9 %copy-start.10 = (bf16[128,32]{0,1:T(8,128)(2,1)S(1)}, bf16[128,32]{0,1:T(8,128)(2,1)}, u32[]{:S(2)}) copy-start(bf16[128,32]{0,1:T(8,128)(2,1)} %param.22) | copy-start | bytes 24580
  78.6 14.8 %copy-start.12 = (f32[128,2]{0,1:T(2,128)S(1)}, f32[128,2]{0,1:T(2,128)}, u32[]{:S(2)}) copy-start(f32[128,2]{0,1:T(2,128)} %param.33) | copy-start | bytes 3076
  78.6 15.5 %copy-start.2 = (bf16[2048,128]{1,0:T(8,128)(2,1)S(1)}, bf16[2048,128]{1,0:T(8,128)(2,1)}, u32[]{:S(2)}) copy-start(bf16[2048,128]{1,0:T(8,128)(2,1)} %param.37) | copy-start | bytes 1572868
  78.6 15.8 %copy-start.14 = (bf16[2048,128]{1,0:T(8,128)(2,1)S(1)}, bf16[2048,128]{1,0:T(8,128)(2,1)}, u32[]{:S(2)}) copy-start(bf16[2048,128]{1,0:T(8,128)(2,1)} %param.38) | copy-start | bytes 1572868
  80.5 25.0 %copy-start.7 = (bf16[512,256]{1,0:T(8,128)(2,1)S(1)}, bf16[512,256]{1,0:T(8,128)(2,1)}, u32[]{:S(2)}) copy-start(bf16[512,256]{1,0:T(8,128)(2,1)} %param.27) | copy-start | bytes 786436
  94.1 10.7 %copy-start.15 = (bf16[1536,128]{1,0:T(8,128)(2,1)S(1)}, bf16[1536,128]{1,0:T(8,128)(2,1)}, u32[]{:S(2)}) copy-start(bf16[1536,128]{1,0:T(8,128)(2,1)} %param.26) | copy-start | bytes 1179652
  109.8 1.2 copy-start.1
  109.8 1.3 copy-start.8
  127.5 17.1 %all-to-all-start.1 = ((bf16[8,48,512]{2,1,0:T(8,128)(2,1)}), bf16[8,48,512]{2,1,0:T(8,128)(2,1)S(1)}, u32[]{:S(2)}, u32[]{:S(2)}) async-start(bf16[8,48,512]{2,1,0:T(8,128)(2,1)} %bitcast.78), calls=%async_computation.1 | async-start | bytes 786432 | tf_op jit(solution)/shard_map/all_to_all | solution.py:182
  142.7 3.6 %copy-start.9 = (f32[128,2]{1,0:T(8,128)S(1)}, f32[128,2]{1,0:T(8,128)}, u32[]{:S(2)}) copy-start(f32[128,2]{1,0:T(8,128)} %copy.30) | copy-start | bytes 3076
  143.7 3.3 %copy-start.3 = (bf16[512,512]{1,0:T(8,128)(2,1)S(1)}, bf16[512,512]{1,0:T(8,128)(2,1)}, u32[]{:S(2)}) copy-start(bf16[512,512]{1,0:T(8,128)(2,1)} %param.39) | copy-start | bytes 1572868
  143.7 3.3 %copy-start.5 = (bf16[128,512]{1,0:T(8,128)(2,1)S(1)}, bf16[128,512]{1,0:T(8,128)(2,1)}, u32[]{:S(2)}) copy-start(bf16[128,512]{1,0:T(8,128)(2,1)} %all_gather.18) | copy-start | bytes 393220
Sparse Core Ops, SparseCore 0:
  28.3 37.9 all-gather.2
  78.7 43.0 all-gather.4
where the time goes:
time: 155 us
  waiting for transfers between devices  55.7 us (36%)
  blocking collectives  31.1 us (20%)
  matrix products  24.2 us (16%)
  between operations  14.4 us (9%)
  starting transfers between devices  11.2 us (7%)
  local copies, waits for them, and re-layouts  9.52 us (6%)
  other arithmetic  8.67 us (6%)
    all_to_all x1, waiting for transfers between devices, per_device(): lax.all_to_all(outgoing, 'ep', split_axis=0, concat_axis=0, tiled=True)  45.2 us
    all_gather x1, blocking collectives, per_device(): lax.all_gather(rotary_key, 'ep', axis=0, tiled=True)  12.8 us
    all_gather x1, waiting for transfers between devices, per_device(): lax.all_gather(hidden, 'tp', axis=1, tiled=True)  9.5 us
    all_gather x1, blocking collectives, per_device(): lax.all_gather(shared_hidden, 'tp', axis=1, tiled=True)  9.33 us
    all_gather x1, blocking collectives, per_device(): all_heads = lax.all_gather(heads_out, 'tp', axis=1, tiled=True)  8.93 us
    all_to_all x1, starting transfers between devices, per_device(): lax.all_to_all(outgoing, 'ep', split_axis=0, concat_axis=0, tiled=True)  6.49 us
    dot_general x1, matrix products, per_device(): jnp.dot(all_hidden, expert_down[0], preferred_element_type=jnp.float32)  5.67 us
    all_to_all x1, starting transfers between devices, per_device(): lax.all_to_all(expert_rows.reshape(experts, capacity, features), 'ep', sp...  4.62 us
  transfers between devices with their start and end apart: 4, of which 3 were waited for; matrix products, arithmetic and copies ran while one was open for 14% of the time, Pallas kernels for 0%

commit v1 on v0

--- a/solution.py
+++ b/solution.py
@@ -173,7 +173,7 @@
     ).astype(jnp.bfloat16)
     all_hidden, all_shared = (
         lax.all_gather(hidden, "tp", axis=1, tiled=True),
-        lax.all_gather(shared_hidden, "tp", axis=1, tiled=True),
+        jnp.concatenate(lax.all_gather(shared_hidden, "tp"), axis=1),
     )
     expert_rows = jnp.dot(all_hidden, expert_down[0], preferred_element_type=jnp.float32).astype(
         jnp.bfloat16

time: 155 us -> 155 us (level)
  transfers between devices with their start and end apart: 4 -> 4, of which waited for: 3 -> 3; matrix products, arithmetic and copies ran while one was open for 14% -> 15% of each run, Pallas kernels for 0% -> 0%
where the time goes in v1:
time: 155 us
  waiting for transfers between devices  54.8 us (35%)
  blocking collectives  30.3 us (20%)
  matrix products  25.2 us (16%)
  between operations  14.4 us (9%)
  starting transfers between devices  11.2 us (7%)
  local copies, waits for them, and re-layouts  10.3 us (7%)
  other arithmetic  8.67 us (6%)
    all_to_all x1, waiting for transfers between devices, per_device(): lax.all_to_all(outgoing, 'ep', split_axis=0, concat_axis=0, tiled=True)  45.2 us
    all_gather x1, blocking collectives, per_device(): lax.all_gather(rotary_key, 'ep', axis=0, tiled=True)  12.7 us
    all_gather x1, blocking collectives, per_device(): all_heads = lax.all_gather(heads_out, 'tp', axis=1, tiled=True)  8.94 us
    all_gather x1, waiting for transfers between devices, per_device(): lax.all_gather(hidden, 'tp', axis=1, tiled=True)  8.65 us
    all_gather x1, blocking collectives, per_device(): lax.all_gather(shared_hidden, 'tp')  8.64 us
    all_to_all x1, starting transfers between devices, per_device(): lax.all_to_all(outgoing, 'ep', split_axis=0, concat_axis=0, tiled=True)  6.49 us
    dot_general x1, matrix products, per_device(): jnp.dot(all_hidden, expert_down[0], preferred_element_type=jnp.float32)  5.67 us
    all_to_all x1, starting transfers between devices, per_device(): lax.all_to_all(expert_rows.reshape(experts, capacity, features), 'ep', sp...  4.6 us
  transfers between devices with their start and end apart: 4, of which 3 were waited for; matrix products, arithmetic and copies ran while one was open for 15% of the time, Pallas kernels for 0%

profile of v1, /device:TPU:0, one launch (start us, length us, event | category | flops | bytes accessed | tf_op | source)
XLA Modules:
  0.0 154.8 jit_solution(18038828729426986537)
XLA Ops:
  10.2 1.4 scatter_custom_fusion
  11.7 1.2 convert_reduce_fusion
  12.9 1.3 fusion.21
  14.2 1.4 fusion.23
  15.7 3.1 %gather_fusion = bf16[384,2048]{1,0:T(8,128)(2,1)} fusion(bf16[129,2048]{1,0:T(8,128)(2,1)S(1)} %concatenate.12, s32[1024]{0:T(1024)S(1)} %pad_clamp_fusion.1), kind=kCustom, calls=%fused_computation | custom fusion | bytes 3147264 | tf_op jit(solution)/shard_map/gather | solution.py:162
  18.8 6.5 %all-to-all-start = ((bf16[8,48,2048]{2,1,0:T(8,128)(2,1)}), bf16[8,48,2048]{2,1,0:T(8,128)(2,1)S(1)}, u32[]{:S(2)}, u32[]{:S(2)}) async-start(bf16[8,48,2048]{2,1,0:T(8,128)(2,1)} %bitcast.17), calls=%async_computation | async-start | bytes 3145728 | tf_op jit(solution)/shard_map/all_to_all | solution.py:163
  26.3 45.2 %all-to-all-done = bf16[8,48,2048]{2,1,0:T(8,128)(2,1)S(1)} async-done(((bf16[8,48,2048]{2,1,0:T(8,128)(2,1)}), bf16[8,48,2048]{2,1,0:T(8,128)(2,1)S(1)}, u32[]{:S(2)}, u32[]{:S(2)}) %all-to-all-start) | async-done | bytes 1572896 | tf_op jit(solution)/shard_map/all_to_all | solution.py:163
  71.5 4.1 %fusion.4 = f32[384,1024]{1,0:T(8,128)S(1)} fusion(bf16[384,2048]{1,0:T(8,128)(2,1)S(1)} %bitcast.80, bf16[1,2048,1024]{2,1,0:T(8,128)(2,1)} %param.34), kind=kOutput, calls=%fused_computation.7 | convolution fusion | flops 1610612736 | bytes 7340032 | tf_op jit(solution)/shard_map/dot_general | solution.py:167
  75.7 2.9 %multiply_convert_fusion = bf16[384,1024]{1,0:T(8,128)(2,1)} fusion(f32[384,1024]{1,0:T(8,128)S(1)} %fusion.4, bf16[384,2048]{1,0:T(8,128)(2,1)S(1)} %bitcast.81, bf16[1,2048,1024]{2,1,0:T(8,128)(2,1)S(1)} %copy-done.13), kind=kOutput, calls=%fused_computation.14 | convolution fusion | flops 1612972032 | bytes 8126464 | tf_op jit(solution)/shard_map/dot_general | solution.py:168
  78.8 1.6 %convolution_convert_fusion.3 = bf16[128,256]{1,0:T(8,128)(2,1)S(1)} fusion(bf16[1536,256]{1,0:T(8,128)(2,1)} %param.25, bf16[128,1536]{1,0:T(8,128)(2,1)S(1)} %copy-done.6, f32[1536]{0:T(1024)S(1)} %copy-done.15, f32[128]{0:T(128)S(1)} %add_rsqrt_fusion.2), kind=kOutput, calls=%fused_computation.28 | convolution fusion | flops 101482496 | bytes 1251840 | tf_op jit(solution)/shard_map/dot_general | solution.py:77
  80.5 12.7 %all_gather.19 = bf16[1024,32]{0,1:T(8,128)(2,1)S(1)} all-gather(bf16[128,32]{0,1:T(8,128)(2,1)S(1)} %copy-done.10), channel_id=1, replica_groups=mesh['ep'=8,'tp'=4] {'ep'}, dimensions={0}, use_global_device_ids=true | all-gather | bytes 73728 | tf_op jit(solution)/shard_map/all_gather | solution.py:128
  94.6 8.6 %all-gather = bf16[512,128]{1,0:T(8,128)(2,1)S(1)} all-gather(bf16[128,128]{1,0:T(8,128)(2,1)S(1)} %fusion.20), channel_id=2, replica_groups=mesh['ep'=8,'tp'=4] {'tp'}, dimensions={0}, use_global_device_ids=true | all-gather | bytes 163840 | tf_op jit(solution)/shard_map/all_gather | solution.py:176
  104.7 1.4 fusion.34
  106.5 1.7 %convolution_convert_fusion.1 = bf16[1024,256]{0,1:T(8,128)(2,1)S(1)} fusion(bf16[1024,512]{1,0:T(8,128)(2,1)} %all-gather.4.cloned.1.call-done, bf16[512,256]{1,0:T(8,128)(2,1)S(1)} %copy-done.7), kind=kOutput, calls=%fused_computation.18 | convolution fusion | flops 268697600 | bytes 1835008 | tf_op jit(solution)/shard_map/while/body/eval_jaxpr/dot_general | solution.py:116
  108.7 2.0 %fusion.51 = (f32[4,128]{1,0:T(4,128)S(1)}, f32[4,128,1024]{2,1,0:T(8,128)S(1)}) fusion(f32[4,128,1024]{2,1,0:T(8,128)S(1)} %fusion.52, f32[128,4,16]{0,2,1:T(8,128)S(1)} %get-tuple-element.27, f32[128,4,16]{0,2,1:T(8,128)S(1)} %get-tuple-element.26, f32[1024,16]{0,1:T(8,128)S(1)} %get-tuple-element.25, f32[1024,16]{0,1:T(8,128)S(1)} %get-tuple-element.24), kind=kOutput, calls=%fused_computation.94 | convolution fusion | flops 202948096 | bytes 4392960 | tf_op jit(solution)/shard_map/while/body/eval_jaxpr/qhr,kr->hqk/dot_general | solution.py:100
  112.0 1.3 convolution_convert_fusion
  113.3 8.6 %all-gather.6.cloned.1.call-done = bf16[384,4096]{1,0:T(8,128)(2,1)} async-done(((bf16[384,1024]{1,0:T(8,128)(2,1)}), bf16[384,4096]{1,0:T(8,128)(2,1)}) %all-gather.6.cloned.1.call-update) | async-done | bytes 3145744 | tf_op jit(solution)/shard_map/all_gather | solution.py:175
  121.9 5.7 %fusion.11 = bf16[384,512]{1,0:T(8,128)(2,1)} fusion(bf16[384,4096]{1,0:T(8,128)(2,1)} %all-gather.6.cloned.1.call-done, bf16[1,4096,512]{2,1,0:T(8,128)(2,1)} %param.36), kind=kOutput, calls=%fused_computation.19 | convolution fusion | flops 1610809344 | bytes 7733248 | tf_op jit(solution)/shard_map/dot_general | solution.py:178
  127.6 4.6 %all-to-all-start.1 = ((bf16[8,48,512]{2,1,0:T(8,128)(2,1)}), bf16[8,48,512]{2,1,0:T(8,128)(2,1)S(1)}, u32[]{:S(2)}, u32[]{:S(2)}) async-start(bf16[8,48,512]{2,1,0:T(8,128)(2,1)} %bitcast.84), calls=%async_computation.1 | async-start | bytes 786432 | tf_op jit(solution)/shard_map/all_to_all | solution.py:182
  132.2 1.6 %fusion.19 = bf16[128,4,64]{0,2,1:T(8,128)(2,1)S(1)} fusion(bf16[1024,4,64]{0,2,1:T(8,128)(2,1)} %bitcast.78, f32[4,128,1024]{2,1,0:T(8,128)S(1)} %get-tuple-element.44, f32[4,128]{1,0:T(4,128)S(1)} %get-tuple-element.29, f32[128,4]{0,1:T(4,128)S(1)} %bitcast_add_fusion.1, f32[128,4]{0,1:T(4,128)S(1)} %get-tuple-element.28), kind=kOutput, calls=%fused_computation.29 | convolution fusion | flops 68255744 | bytes 2693120 | tf_op jit(solution)/shard_map/while/body/eval_jaxpr/hqk,khe->hqe/dot_general | solution.py:106
  133.8 8.9 %all_gather.20 = bf16[128,1024]{0,1:T(8,128)(2,1)S(1)} all-gather(bf16[128,256]{0,1:T(8,128)(2,1)S(1)} %bitcast.85), channel_id=1, replica_groups=mesh['ep'=8,'tp'=4] {'tp'}, dimensions={1}, use_global_device_ids=true | all-gather | bytes 327680 | tf_op jit(solution)/shard_map/all_gather | solution.py:138
  142.8 1.0 convolution_convert_fusion.2
  143.8 0.9 all-to-all-done.1
  144.7 1.3 gather_fusion.1
  (81 shorter events, 11.3 us)
Async XLA Ops:
  7.2 135.6 %copy-start = (bf16[1024,512]{1,0:T(8,128)(2,1)S(1)}, bf16[1024,512]{1,0:T(8,128)(2,1)}, u32[]{:S(2)}) copy-start(bf16[1024,512]{1,0:T(8,128)(2,1)} %param.29) | copy-start | bytes 3145732
  18.8 6.5 %copy-start.4 = (bf16[128,512]{1,0:T(8,128)(2,1)S(1)}, bf16[128,512]{1,0:T(8,128)(2,1)}, u32[]{:S(2)}) copy-start(bf16[128,512]{1,0:T(8,128)(2,1)} %param.21) | copy-start | bytes 393220
  18.8 6.7 %copy-start.11 = (f32[512]{0:T(512)S(1)}, f32[512]{0:T(512)}, u32[]{:S(2)}) copy-start(f32[512]{0:T(512)} %param.24) | copy-start | bytes 6148
  18.8 52.7 %all-to-all-start = ((bf16[8,48,2048]{2,1,0:T(8,128)(2,1)}), bf16[8,48,2048]{2,1,0:T(8,128)(2,1)S(1)}, u32[]{:S(2)}, u32[]{:S(2)}) async-start(bf16[8,48,2048]{2,1,0:T(8,128)(2,1)} %bitcast.17), calls=%async_computation | async-start | bytes 3145728 | tf_op jit(solution)/shard_map/all_to_all | solution.py:163
  25.3 81.2 %all-gather.4.cloned.1.call-start = ((), (), s32[]{:S(2)}) async-start(), calls=%async_computation.2 | async-start | bytes 1179648 | tf_op jit(solution)/shard_map/all_gather | solution.py:127
  26.3 95.6 %all-gather.6.cloned.1.call-start = ((), (), s32[]{:S(2)}) async-start(), calls=%async_computation.3 | async-start | bytes 3932160 | tf_op jit(solution)/shard_map/all_gather | solution.py:175
  71.5 4.2 %copy-start.13 = (bf16[1,2048,1024]{2,1,0:T(8,128)(2,1)S(1)}, bf16[1,2048,1024]{2,1,0:T(8,128)(2,1)}, u32[]{:S(2)}) copy-start(bf16[1,2048,1024]{2,1,0:T(8,128)(2,1)} %param.35) | copy-start | bytes 12582916
  75.7 2.9 %copy-start.6 = (bf16[128,1536]{1,0:T(8,128)(2,1)S(1)}, bf16[128,1536]{1,0:T(8,128)(2,1)}, u32[]{:S(2)}) copy-start(bf16[128,1536]{1,0:T(8,128)(2,1)} %param.20) | copy-start | bytes 1179652
  75.7 3.1 %copy-start.15 = (f32[1536]{0:T(1024)S(1)}, f32[1536]{0:T(1024)}, u32[]{:S(2)}) copy-start(f32[1536]{0:T(1024)} %param.23) | copy-start | bytes 18436
  78.6 1.9 %copy-start.10 = (bf16[128,32]{0,1:T(8,128)(2,1)S(1)}, bf16[128,32]{0,1:T(8,128)(2,1)}, u32[]{:S(2)}) copy-start(bf16[128,32]{0,1:T(8,128)(2,1)} %param.22) | copy-start | bytes 24580
  78.6 14.7 %copy-start.12 = (f32[128,2]{0,1:T(2,128)S(1)}, f32[128,2]{0,1:T(2,128)}, u32[]{:S(2)}) copy-start(f32[128,2]{0,1:T(2,128)} %param.33) | copy-start | bytes 3076
  78.6 15.4 %copy-start.2 = (bf16[2048,128]{1,0:T(8,128)(2,1)S(1)}, bf16[2048,128]{1,0:T(8,128)(2,1)}, u32[]{:S(2)}) copy-start(bf16[2048,128]{1,0:T(8,128)(2,1)} %param.37) | copy-start | bytes 1572868
  78.6 15.7 %copy-start.14 = (bf16[2048,128]{1,0:T(8,128)(2,1)S(1)}, bf16[2048,128]{1,0:T(8,128)(2,1)}, u32[]{:S(2)}) copy-start(bf16[2048,128]{1,0:T(8,128)(2,1)} %param.38) | copy-start | bytes 1572868
  93.3 13.2 %copy-start.7 = (bf16[512,256]{1,0:T(8,128)(2,1)S(1)}, bf16[512,256]{1,0:T(8,128)(2,1)}, u32[]{:S(2)}) copy-start(bf16[512,256]{1,0:T(8,128)(2,1)} %param.27) | copy-start | bytes 786436
  110.7 1.2 copy-start.1
  110.7 1.3 copy-start.8
  127.6 17.1 %all-to-all-start.1 = ((bf16[8,48,512]{2,1,0:T(8,128)(2,1)}), bf16[8,48,512]{2,1,0:T(8,128)(2,1)S(1)}, u32[]{:S(2)}, u32[]{:S(2)}) async-start(bf16[8,48,512]{2,1,0:T(8,128)(2,1)} %bitcast.84), calls=%async_computation.1 | async-start | bytes 786432 | tf_op jit(solution)/shard_map/all_to_all | solution.py:182
  142.8 3.6 %copy-start.9 = (f32[128,2]{1,0:T(8,128)S(1)}, f32[128,2]{1,0:T(8,128)}, u32[]{:S(2)}) copy-start(f32[128,2]{1,0:T(8,128)} %copy.31) | copy-start | bytes 3076
  143.8 3.3 %copy-start.3 = (bf16[512,512]{1,0:T(8,128)(2,1)S(1)}, bf16[512,512]{1,0:T(8,128)(2,1)}, u32[]{:S(2)}) copy-start(bf16[512,512]{1,0:T(8,128)(2,1)} %param.39) | copy-start | bytes 1572868
  143.8 3.3 %copy-start.5 = (bf16[4,128,128]{1,2,0:T(8,128)(2,1)S(1)}, bf16[4,128,128]{1,2,0:T(8,128)(2,1)}, u32[]{:S(2)}) copy-start(bf16[4,128,128]{1,2,0:T(8,128)(2,1)} %copy.27) | copy-start | bytes 393220
Sparse Core Ops, SparseCore 0:
  28.3 37.9 all-gather.3
  78.7 43.1 all-gather.5
